TPU v7x, 512 devices: a whole 4x8x8 slice. The times are simulated.
512 devices in a mesh: row: 32 (over z, x), col: 16 (over y, core).
Axes of the slice: x: 4, y: 8, z: 8, core: 2. Of those that a mesh axis runs over, the one named last changes fastest.
Arguments:
- tokens: bfloat16 [32768, 2048], P('row'), may hold values from -136 to 136
- norm_gain: float32 [2048], replicated, may hold values from 0.1 to 1.9
- w_in: bfloat16 [2048, 1024], P(None, 'col'), may hold values from -0.125 to 0.125
- w_out: bfloat16 [1024, 2048], P(None, 'col'), may hold values from -0.1875 to 0.1875
Outputs:
- mixed_tokens: bfloat16 [32768, 2048], P('row', 'col')
All inputs are finite; a program needn't handle non-finite values.
Results may differ from a plain program's by a relative error of at most 0.013.
Values may be sent and summed in bfloat16 or wider, within the bound.
No kernel may reach another device: no remote copies, remote signals or barrier semaphores. Data moves between devices by JAX's collectives and lax.ppermute only.
A program may use at most 64 MiB of HBM per device.

v0:
```python
import math
import jax
import jax.numpy as jnp
from jax import lax
from jax.sharding import PartitionSpec as P

GROUP = 256
NORM_EPS = 1e-06


def in_one_piece(arrays, axis, split_dim, concat_dim, along):
    ends, at = ([], 0)
    for a in arrays[:-1]:
        at += a.shape[along]
        ends.append(at)
    both = jnp.concatenate(arrays, axis=along)
    return tuple(
        jnp.split(
            lax.all_to_all(both, axis, split_axis=split_dim, concat_axis=concat_dim, tiled=True),
            ends,
            axis=along,
        )
    )


def as_sent(array):

    def short(part):
        return part.astype(jnp.bfloat16) if part.dtype == jnp.float32 else part

    return jax.tree.map(short, array)


def rotation_table(first_index, second_index, spectral_magnitude, factor):
    phase = (first_index * second_index % spectral_magnitude).astype(jnp.float32) * (
        2.0 * math.pi / spectral_magnitude
    )
    return (jnp.cos(phase) * factor, jnp.sin(phase) * factor)


def twiddle(real_input_values, imag_in, freq_index, pos_index, spectral_magnitude):
    cosine, sine = rotation_table(freq_index, pos_index, spectral_magnitude, 1.0)
    return (
        real_input_values * cosine + imag_in * sine,
        imag_in * cosine - real_input_values * sine,
    )


def second_section(stacked, half):
    length_dev = stacked.shape[1]
    stride = min(length_dev, 512)
    positions = lax.broadcasted_iota(jnp.int32, (length_dev, stride), 0)
    real_blocks = []
    imag_blocks = []
    for offset in range(0, length_dev, stride):
        freqs = lax.broadcasted_iota(jnp.int32, (length_dev, stride), 1) + offset
        cosine, sine = rotation_table(positions, freqs, length_dev, 1.0)
        with_cos = jnp.dot(stacked, cosine, precision=lax.Precision.HIGH)
        with_sin = jnp.dot(stacked, sine, precision=lax.Precision.HIGH)
        real_blocks.append(with_cos[:half] + with_sin[half:])
        imag_blocks.append(with_cos[half:] - with_sin[:half])
    return (jnp.concatenate(real_blocks, 1), jnp.concatenate(imag_blocks, 1))


def reorder_positions(arrived):
    channels, row_count, _, block_len = arrived.shape
    return jnp.swapaxes(arrived.reshape(channels, row_count, block_len), 1, 2).reshape(
        channels, row_count * block_len
    )


def local(tokens, norm_gain, w_in, w_out):
    length_dev = tokens.shape[0]
    row_count = lax.axis_size("row")
    col_count = lax.axis_size("col")
    total_len = length_dev * row_count
    widened = tokens.astype(jnp.float32)
    inverse = lax.rsqrt(jnp.mean(widened * widened, axis=1, keepdims=True) + NORM_EPS)
    normed = (widened * inverse * norm_gain[None, :]).astype(jnp.bfloat16)
    projected = lax.dot_general(
        w_in, normed, (((0,), (1,)), ((), ())), preferred_element_type=jnp.float32
    ).astype(jnp.bfloat16)
    channels = projected.shape[0]
    block_len = length_dev // row_count
    small_cos, small_sin = rotation_table(
        lax.broadcasted_iota(jnp.int32, (row_count, row_count), 0),
        lax.broadcasted_iota(jnp.int32, (row_count, row_count), 1),
        row_count,
        1.0 / math.sqrt(total_len),
    )
    per_row = channels // row_count
    arrived = lax.all_to_all(
        projected.reshape(channels, 1, length_dev), "row", split_axis=0, concat_axis=1, tiled=True
    )
    values = arrived.astype(jnp.float32)
    real_one = jnp.einsum("ka,cab->ckb", small_cos, values, precision=lax.Precision.HIGH)
    imag_one = -jnp.einsum("ka,cab->ckb", small_sin, values, precision=lax.Precision.HIGH)
    freq_index = lax.broadcasted_iota(jnp.int32, (row_count, length_dev), 0)
    pos_index = lax.broadcasted_iota(jnp.int32, (row_count, length_dev), 1)
    real_two, imag_two = twiddle(real_one, imag_one, freq_index, pos_index, total_len)
    stacked = jnp.concatenate(
        [
            real_two.reshape(per_row * row_count, length_dev),
            imag_two.reshape(per_row * row_count, length_dev),
        ],
        0,
    )
    real_three, imag_three = second_section(stacked, per_row * row_count)
    shaped = (per_row, row_count, row_count, block_len)
    back_real, back_imag = tuple(
        (
            part.astype(jnp.float32)
            for part in in_one_piece(
                (
                    real_three.reshape(shaped).astype(jnp.bfloat16),
                    imag_three.reshape(shaped).astype(jnp.bfloat16),
                ),
                "row",
                2,
                0,
                1,
            )
        )
    )
    spec_real = reorder_positions(back_real)
    spec_imag = reorder_positions(back_imag)
    quarter = length_dev // col_count
    group_cosine_table, group_sine_table = rotation_table(
        lax.broadcasted_iota(jnp.int32, (GROUP, GROUP), 0),
        lax.broadcasted_iota(jnp.int32, (GROUP, GROUP), 1),
        GROUP,
        1.0 / math.sqrt(GROUP),
    )
    real_input_values = lax.all_to_all(
        as_sent(spec_real.reshape(channels, col_count, quarter)),
        "col",
        split_axis=1,
        concat_axis=0,
        tiled=True,
    )
    imag_in = lax.all_to_all(
        as_sent(spec_imag.reshape(channels, col_count, quarter)),
        "col",
        split_axis=1,
        concat_axis=0,
        tiled=True,
    )
    width_all = real_input_values.shape[0]
    item_count = real_input_values.shape[2]
    groups = width_all // GROUP
    real_by_group = real_input_values.reshape(groups, GROUP, item_count)
    imaginary_by_group = imag_in.reshape(groups, GROUP, item_count)
    merged_spectrum = jnp.einsum(
        "hz,azo->aho", group_cosine_table, real_by_group, precision=lax.Precision.HIGH
    )
    merged_spectrum = merged_spectrum + jnp.einsum(
        "hz,azo->aho", group_sine_table, imaginary_by_group, precision=lax.Precision.HIGH
    )
    result = merged_spectrum.reshape(width_all, 1, item_count).astype(jnp.bfloat16)
    portion = lax.all_gather(result, "col", axis=2, tiled=True)
    flat = portion.reshape(portion.shape[0], portion.shape[2])
    output = lax.dot_general(
        flat, w_out, (((0,), (0,)), ((), ())), preferred_element_type=jnp.float32
    )
    return output.astype(jnp.bfloat16)


def solution(mesh):
    placed = (P("row", None), P(), P(None, "col"), P(None, "col"))
    return jax.shard_map(
        local, mesh=mesh, in_specs=placed, out_specs=P("row", "col"), check_vma=False
    )
```

profile of v0, /device:TPU:1, one launch (start us, length us, event | category | flops | bytes accessed | tf_op | source)
XLA Modules:
  0.0 170.5 jit_solution(13047247857492114618)
XLA Ops:
  6.5 3.2 %fusion = f32[1024]{0:T(1024)S(1)} fusion(bf16[1024,2048]{1,0:T(8,128)(2,1)} %param.4), kind=kLoop, calls=%fused_computation.2 | loop fusion | flops 6290432 | bytes 4198400 | tf_op jit(solution)/shard_map/reduce_sum | solution.py:78
  9.8 0.3 copy-done.1
  10.0 2.4 %fusion.38 = bf16[64,1,1024]{2,0,1:T(8,128)(2,1)S(1)} fusion(bf16[2048,64]{0,1:T(8,128)(2,1)} %param.6, bf16[1024,2048]{1,0:T(8,128)(2,1)S(1)} %copy-done.1, f32[2048]{0:T(1024)S(1)} %copy-done.2, f32[1024]{0:T(1024)S(1)} %add_rsqrt_fusion), kind=kOutput, calls=%fused_computation.44 | convolution fusion | flops 276889600 | bytes 4599808 | tf_op jit(solution)/shard_map/dot_general | solution.py:80
  12.4 0.5 broadcast.165
  13.0 0.7 reduce.1
  13.6 0.7 reshape.90
  14.3 13.9 %all-to-all-start = ((bf16[32,2,1024]{2,1,0:T(2,128)(2,1)}), bf16[32,2,1024]{2,1,0:T(2,128)(2,1)S(1)}, u32[]{:S(2)}, u32[]{:S(2)}) async-start(bf16[32,2,1024]{2,1,0:T(2,128)(2,1)} %reshape.90), calls=%async_computation | async-start | bytes 262144 | tf_op jit(solution)/shard_map/all_to_all | solution.py:92
  28.2 0.5 fusion.78
  28.8 8.6 %all-to-all-done = bf16[32,2,1024]{2,1,0:T(2,128)(2,1)S(1)} async-done(((bf16[32,2,1024]{2,1,0:T(2,128)(2,1)}), bf16[32,2,1024]{2,1,0:T(2,128)(2,1)S(1)}, u32[]{:S(2)}, u32[]{:S(2)}) %all-to-all-start) | async-done | bytes 131104 | tf_op jit(solution)/shard_map/all_to_all | solution.py:92
  37.4 0.1 reshape.91
  37.5 0.7 reduce
  38.3 0.1 all_to_all.49
  38.3 0.3 convolution_bitcast_fusion
  38.6 0.3 multiply_add_fusion
  38.9 8.7 %fusion.21 = f32[128,512]{1,0:T(8,128)S(1)} fusion(f32[64,1024]{1,0:T(8,128)S(1)} %bitcast.98, f32[64,1024]{1,0:T(8,128)S(1)} %bitcast.94), kind=kOutput, calls=%fused_computation.28 | convolution fusion | flops 410124288 | bytes 786432 | tf_op jit(solution)/shard_map/dot_general | solution.py:59
  47.6 8.6 %fusion.17 = f32[128,512]{1,0:T(8,128)S(1)} fusion(s32[512]{0:T(512)S(1)} %iota_add_fusion, f32[64,1024]{1,0:T(8,128)S(1)} %bitcast.99, f32[64,1024]{1,0:T(8,128)S(1)} %bitcast.95), kind=kOutput, calls=%fused_computation.24 | convolution fusion | flops 410124288 | bytes 788480 | tf_op jit(solution)/shard_map/dot_general | solution.py:58
  56.2 8.9 %fusion.15 = f32[128,512]{1,0:T(8,128)S(1)} fusion(s32[512]{0:T(512)S(1)} %iota_add_fusion, f32[64,1024]{1,0:T(8,128)S(1)} %bitcast.100, f32[64,1024]{1,0:T(8,128)S(1)} %bitcast.96), kind=kOutput, calls=%fused_computation.22 | convolution fusion | flops 410124288 | bytes 788480 | tf_op jit(solution)/shard_map/dot_general | solution.py:59
  65.1 8.6 %fusion.23 = f32[128,512]{1,0:T(8,128)S(1)} fusion(f32[64,1024]{1,0:T(8,128)S(1)} %bitcast.101, f32[64,1024]{1,0:T(8,128)S(1)} %bitcast.97), kind=kOutput, calls=%fused_computation.30 | convolution fusion | flops 410124288 | bytes 786432 | tf_op jit(solution)/shard_map/dot_general | solution.py:58
  73.9 0.4 convert_element_type.108
  74.2 0.7 copy.35
  74.9 0.4 convert_element_type.107
  75.3 0.7 copy.34
  75.9 0.3 fusion.136
  76.2 0.4 reshape.92
  76.6 13.7 %all_to_all.66 = bf16[32,2,2048]{2,1,0:T(2,128)(2,1)S(1)} all-to-all(bf16[32,2,2048]{2,1,0:T(2,128)(2,1)S(1)} %reshape.92), channel_id=1, replica_groups=mesh['row'=32,'col'=16] {'row'}, dimensions={0} | all-to-all | bytes 524288 | tf_op jit(solution)/shard_map/all_to_all | solution.py:19
  90.3 0.4 reshape.93
  90.7 0.2 slice_bitcast_fusion
  90.9 0.6 copy.41
  91.5 0.9 reshape.96
  92.4 10.9 %all-to-all-start.3 = ((bf16[16,2,2048]{2,1,0:T(2,128)(2,1)}), bf16[16,2,2048]{2,1,0:T(2,128)(2,1)S(1)}, u32[]{:S(2)}, u32[]{:S(2)}) async-start(bf16[16,2,2048]{2,1,0:T(2,128)(2,1)} %reshape.96), calls=%async_computation.3 | async-start | bytes 262144 | tf_op jit(solution)/shard_map/all_to_all | solution.py:141
  103.3 0.6 copy.37
  103.9 0.9 reshape.94
  104.8 7.4 %all-to-all-done.3 = bf16[16,2,2048]{2,1,0:T(2,128)(2,1)S(1)} async-done(((bf16[16,2,2048]{2,1,0:T(2,128)(2,1)}), bf16[16,2,2048]{2,1,0:T(2,128)(2,1)S(1)}, u32[]{:S(2)}, u32[]{:S(2)}) %all-to-all-start.3) | async-done | bytes 131104 | tf_op jit(solution)/shard_map/all_to_all | solution.py:141
  112.2 3.4 %all-to-all-start.2 = ((bf16[16,2,2048]{2,1,0:T(2,128)(2,1)}), bf16[16,2,2048]{2,1,0:T(2,128)(2,1)S(1)}, u32[]{:S(2)}, u32[]{:S(2)}) async-start(bf16[16,2,2048]{2,1,0:T(2,128)(2,1)} %reshape.94), calls=%async_computation.2 | async-start | bytes 262144 | tf_op jit(solution)/shard_map/all_to_all | solution.py:134
  115.6 0.0 all-gather.2.cloned.1.call-start
  115.6 0.2 reshape.97
  115.9 0.2 copy.42
  116.1 0.2 reshape.83
  116.3 8.2 %all-to-all-done.2 = bf16[16,2,2048]{2,1,0:T(2,128)(2,1)S(1)} async-done(((bf16[16,2,2048]{2,1,0:T(2,128)(2,1)}), bf16[16,2,2048]{2,1,0:T(2,128)(2,1)S(1)}, u32[]{:S(2)}, u32[]{:S(2)}) %all-to-all-start.2) | async-done | bytes 131104 | tf_op jit(solution)/shard_map/all_to_all | solution.py:134
  124.5 0.2 reshape.95
  124.8 0.2 copy.38
  125.0 0.2 reshape.82
  125.2 1.2 fusion.49
  126.4 1.2 fusion.37
  127.6 0.1 copy.44
  127.7 0.7 convert_element_type.118
  128.5 32.2 %all-gather.2.cloned.1.call-done = bf16[1024,1,1024]{0,2,1:T(8,128)(2,1)} async-done(((bf16[1024,1,64]{0,2,1:T(8,128)(2,1)}), bf16[1024,1,1024]{0,2,1:T(8,128)(2,1)}) %all-gather.2.cloned.1.call-update) | async-done | bytes 2097168 | tf_op jit(solution)/shard_map/all_gather | solution.py:160
  160.7 3.0 %fusion.29 = bf16[1024,128]{1,0:T(8,128)(2,1)} fusion(bf16[1024,128]{1,0:T(8,128)(2,1)S(1)} %copy-done, bf16[1024,1,1024]{0,2,1:T(8,128)(2,1)} %all-gather.2.cloned.1.call-done), kind=kOutput, calls=%fused_computation.36 | convolution fusion | flops 268566528 | bytes 2621440 | tf_op jit(solution)/shard_map/dot_general | solution.py:162
  (16 shorter events, 0.2 us)
Async XLA Ops:
  6.5 154.2 %copy-start = (bf16[1024,128]{1,0:T(8,128)(2,1)S(1)}, bf16[1024,128]{1,0:T(8,128)(2,1)}, u32[]{:S(2)}) copy-start(bf16[1024,128]{1,0:T(8,128)(2,1)} %param.7) | copy-start | bytes 786436
  6.5 3.5 %copy-start.1 = (bf16[1024,2048]{1,0:T(8,128)(2,1)S(1)}, bf16[1024,2048]{1,0:T(8,128)(2,1)}, u32[]{:S(2)}) copy-start(bf16[1024,2048]{1,0:T(8,128)(2,1)} %param.4) | copy-start | bytes 12582916
  6.5 3.5 %copy-start.2 = (f32[2048]{0:T(1024)S(1)}, f32[2048]{0:T(1024)}, u32[]{:S(2)}) copy-start(f32[2048]{0:T(1024)} %param.5) | copy-start | bytes 24580
  14.3 23.1 %all-to-all-start = ((bf16[32,2,1024]{2,1,0:T(2,128)(2,1)}), bf16[32,2,1024]{2,1,0:T(2,128)(2,1)S(1)}, u32[]{:S(2)}, u32[]{:S(2)}) async-start(bf16[32,2,1024]{2,1,0:T(2,128)(2,1)} %reshape.90), calls=%async_computation | async-start | bytes 262144 | tf_op jit(solution)/shard_map/all_to_all | solution.py:92
  92.4 19.8 %all-to-all-start.3 = ((bf16[16,2,2048]{2,1,0:T(2,128)(2,1)}), bf16[16,2,2048]{2,1,0:T(2,128)(2,1)S(1)}, u32[]{:S(2)}, u32[]{:S(2)}) async-start(bf16[16,2,2048]{2,1,0:T(2,128)(2,1)} %reshape.96), calls=%async_computation.3 | async-start | bytes 262144 | tf_op jit(solution)/shard_map/all_to_all | solution.py:141
  112.2 12.3 %all-to-all-start.2 = ((bf16[16,2,2048]{2,1,0:T(2,128)(2,1)}), bf16[16,2,2048]{2,1,0:T(2,128)(2,1)S(1)}, u32[]{:S(2)}, u32[]{:S(2)}) async-start(bf16[16,2,2048]{2,1,0:T(2,128)(2,1)} %reshape.94), calls=%async_computation.2 | async-start | bytes 262144 | tf_op jit(solution)/shard_map/all_to_all | solution.py:134
  115.6 45.1 %all-gather.2.cloned.1.call-start = ((), (), s32[]{:S(2)}) async-start(), calls=%async_computation.4 | async-start | bytes 2228224 | tf_op jit(solution)/shard_map/all_gather | solution.py:160
Sparse Core Ops, SparseCore 0:
  128.6 32.0 all-gather.1
where the time goes:
time: 171 us
  waiting for transfers between devices  56.5 us (33%)
  matrix products  43.2 us (25%)
  starting transfers between devices  28.2 us (16%)
  blocking collectives  13.7 us (8%)
  between operations  13.7 us (8%)
  local copies, waits for them, and re-layouts  9.71 us (6%)
  other arithmetic  5.56 us (3%)
    all_gather x1, waiting for transfers between devices, local(): portion = lax.all_gather(result, 'col', axis=2, tiled=True)  32.2 us
    dot_general x2, matrix products, second_section(): with_sin = jnp.dot(stacked, sine, precision=lax.Precision.HIGH)  17.6 us
    dot_general x2, matrix products, second_section(): with_cos = jnp.dot(stacked, cosine, precision=lax.Precision.HIGH)  17.2 us
    all_to_all x1, starting transfers between devices, local(): lax.all_to_all(projected.reshape(channels, 1, length_dev), 'row', split_a...  13.9 us
    all_to_all x1, blocking collectives, in_one_piece(): lax.all_to_all(both, axis, split_axis=split_dim, concat_axis=concat_dim,...  13.7 us
    all_to_all x1, starting transfers between devices, local(): lax.all_to_all(as_sent(spec_imag.reshape(channels, col_count, quarter)),...  10.9 us
    all_to_all x1, waiting for transfers between devices, local(): lax.all_to_all(projected.reshape(channels, 1, length_dev), 'row', split_a...  8.62 us
    all_to_all x1, waiting for transfers between devices, local(): lax.all_to_all(as_sent(spec_real.reshape(channels, col_count, quarter)),...  8.24 us
  transfers between devices with their start and end apart: 4, of which 4 were waited for; matrix products, arithmetic and copies ran while one was open for 2% of the time, Pallas kernels for 0%

commit v1 on v0

--- a/solution.py
+++ b/solution.py
@@ -157,7 +157,7 @@
         "hz,azo->aho", group_sine_table, imaginary_by_group, precision=lax.Precision.HIGH
     )
     result = merged_spectrum.reshape(width_all, 1, item_count).astype(jnp.bfloat16)
-    portion = lax.all_gather(result, "col", axis=2, tiled=True)
+    portion = jnp.concatenate(lax.all_gather(result, "col"), axis=2)
     flat = portion.reshape(portion.shape[0], portion.shape[2])
     output = lax.dot_general(
         flat, w_out, (((0,), (0,)), ((), ())), preferred_element_type=jnp.float32

time: 171 us -> 171 us (level)
  no operation moved by 1% of the time
where the time goes in v1:
time: 171 us
  waiting for transfers between devices  56.5 us (33%)
  matrix products  43.2 us (25%)
  starting transfers between devices  28.2 us (16%)
  blocking collectives  13.7 us (8%)
  between operations  13.7 us (8%)
  local copies, waits for them, and re-layouts  9.71 us (6%)
  other arithmetic  5.56 us (3%)
    all_gather x1, waiting for transfers between devices, local(): portion = jnp.concatenate(lax.all_gather(result, 'col'), axis=2)  32.2 us
    dot_general x2, matrix products, second_section(): with_sin = jnp.dot(stacked, sine, precision=lax.Precision.HIGH)  17.6 us
    dot_general x2, matrix products, second_section(): with_cos = jnp.dot(stacked, cosine, precision=lax.Precision.HIGH)  17.2 us
    all_to_all x1, starting transfers between devices, local(): lax.all_to_all(projected.reshape(channels, 1, length_dev), 'row', split_a...  13.9 us
    all_to_all x1, blocking collectives, in_one_piece(): lax.all_to_all(both, axis, split_axis=split_dim, concat_axis=concat_dim,...  13.7 us
    all_to_all x1, starting transfers between devices, local(): lax.all_to_all(as_sent(spec_imag.reshape(channels, col_count, quarter)),...  10.9 us
    all_to_all x1, waiting for transfers between devices, local(): lax.all_to_all(projected.reshape(channels, 1, length_dev), 'row', split_a...  8.62 us
    all_to_all x1, waiting for transfers between devices, local(): lax.all_to_all(as_sent(spec_real.reshape(channels, col_count, quarter)),...  8.24 us
  transfers between devices with their start and end apart: 4, of which 4 were waited for; matrix products, arithmetic and copies ran while one was open for 2% of the time, Pallas kernels for 0%

profile of v1, /device:TPU:1, one launch (start us, length us, event | category | flops | bytes accessed | tf_op | source)
XLA Modules:
  0.0 170.5 jit_solution(7468568820771376894)
XLA Ops:
  6.5 3.2 %fusion = f32[1024]{0:T(1024)S(1)} fusion(bf16[1024,2048]{1,0:T(8,128)(2,1)} %param.4), kind=kLoop, calls=%fused_computation.2 | loop fusion | flops 6290432 | bytes 4198400 | tf_op jit(solution)/shard_map/reduce_sum | solution.py:78
  9.8 0.3 copy-done.1
  10.0 2.4 %fusion.33 = bf16[64,1,1024]{2,0,1:T(8,128)(2,1)S(1)} fusion(bf16[2048,64]{0,1:T(8,128)(2,1)} %param.6, bf16[1024,2048]{1,0:T(8,128)(2,1)S(1)} %copy-done.1, f32[2048]{0:T(1024)S(1)} %copy-done.2, f32[1024]{0:T(1024)S(1)} %add_rsqrt_fusion), kind=kOutput, calls=%fused_computation.42 | convolution fusion | flops 276889600 | bytes 4599808 | tf_op jit(solution)/shard_map/dot_general | solution.py:80
  12.4 0.5 broadcast.165
  13.0 0.7 reduce.1
  13.6 0.7 reshape.91
  14.3 13.9 %all-to-all-start = ((bf16[32,2,1024]{2,1,0:T(2,128)(2,1)}), bf16[32,2,1024]{2,1,0:T(2,128)(2,1)S(1)}, u32[]{:S(2)}, u32[]{:S(2)}) async-start(bf16[32,2,1024]{2,1,0:T(2,128)(2,1)} %reshape.91), calls=%async_computation | async-start | bytes 262144 | tf_op jit(solution)/shard_map/all_to_all | solution.py:92
  28.2 0.5 fusion.73
  28.8 8.6 %all-to-all-done = bf16[32,2,1024]{2,1,0:T(2,128)(2,1)S(1)} async-done(((bf16[32,2,1024]{2,1,0:T(2,128)(2,1)}), bf16[32,2,1024]{2,1,0:T(2,128)(2,1)S(1)}, u32[]{:S(2)}, u32[]{:S(2)}) %all-to-all-start) | async-done | bytes 131104 | tf_op jit(solution)/shard_map/all_to_all | solution.py:92
  37.4 0.1 reshape.92
  37.5 0.7 reduce
  38.3 0.1 all_to_all.49
  38.3 0.3 convolution_bitcast_fusion
  38.6 0.3 multiply_add_fusion
  38.9 8.7 %fusion.19 = f32[128,512]{1,0:T(8,128)S(1)} fusion(f32[64,1024]{1,0:T(8,128)S(1)} %bitcast.99, f32[64,1024]{1,0:T(8,128)S(1)} %bitcast.95), kind=kOutput, calls=%fused_computation.26 | convolution fusion | flops 410124288 | bytes 786432 | tf_op jit(solution)/shard_map/dot_general | solution.py:59
  47.6 8.6 %fusion.15 = f32[128,512]{1,0:T(8,128)S(1)} fusion(s32[512]{0:T(512)S(1)} %iota_add_fusion, f32[64,1024]{1,0:T(8,128)S(1)} %bitcast.100, f32[64,1024]{1,0:T(8,128)S(1)} %bitcast.96), kind=kOutput, calls=%fused_computation.22 | convolution fusion | flops 410124288 | bytes 788480 | tf_op jit(solution)/shard_map/dot_general | solution.py:58
  56.2 8.9 %fusion.13 = f32[128,512]{1,0:T(8,128)S(1)} fusion(s32[512]{0:T(512)S(1)} %iota_add_fusion, f32[64,1024]{1,0:T(8,128)S(1)} %bitcast.101, f32[64,1024]{1,0:T(8,128)S(1)} %bitcast.97), kind=kOutput, calls=%fused_computation.20 | convolution fusion | flops 410124288 | bytes 788480 | tf_op jit(solution)/shard_map/dot_general | solution.py:59
  65.1 8.6 %fusion.21 = f32[128,512]{1,0:T(8,128)S(1)} fusion(f32[64,1024]{1,0:T(8,128)S(1)} %bitcast.102, f32[64,1024]{1,0:T(8,128)S(1)} %bitcast.98), kind=kOutput, calls=%fused_computation.28 | convolution fusion | flops 410124288 | bytes 786432 | tf_op jit(solution)/shard_map/dot_general | solution.py:58
  73.9 0.4 convert_element_type.109
  74.2 0.7 copy.34
  74.9 0.4 convert_element_type.108
  75.3 0.7 copy.33
  75.9 0.3 fusion.131
  76.2 0.4 reshape.93
  76.6 13.7 %all_to_all.66 = bf16[32,2,2048]{2,1,0:T(2,128)(2,1)S(1)} all-to-all(bf16[32,2,2048]{2,1,0:T(2,128)(2,1)S(1)} %reshape.93), channel_id=1, replica_groups=mesh['row'=32,'col'=16] {'row'}, dimensions={0} | all-to-all | bytes 524288 | tf_op jit(solution)/shard_map/all_to_all | solution.py:19
  90.3 0.4 reshape.94
  90.7 0.2 slice_bitcast_fusion
  90.9 0.6 copy.40
  91.5 0.9 reshape.97
  92.4 10.9 %all-to-all-start.3 = ((bf16[16,2,2048]{2,1,0:T(2,128)(2,1)}), bf16[16,2,2048]{2,1,0:T(2,128)(2,1)S(1)}, u32[]{:S(2)}, u32[]{:S(2)}) async-start(bf16[16,2,2048]{2,1,0:T(2,128)(2,1)} %reshape.97), calls=%async_computation.3 | async-start | bytes 262144 | tf_op jit(solution)/shard_map/all_to_all | solution.py:141
  103.3 0.6 copy.36
  103.9 0.9 reshape.95
  104.8 7.4 %all-to-all-done.3 = bf16[16,2,2048]{2,1,0:T(2,128)(2,1)S(1)} async-done(((bf16[16,2,2048]{2,1,0:T(2,128)(2,1)}), bf16[16,2,2048]{2,1,0:T(2,128)(2,1)S(1)}, u32[]{:S(2)}, u32[]{:S(2)}) %all-to-all-start.3) | async-done | bytes 131104 | tf_op jit(solution)/shard_map/all_to_all | solution.py:141
  112.2 3.4 %all-to-all-start.2 = ((bf16[16,2,2048]{2,1,0:T(2,128)(2,1)}), bf16[16,2,2048]{2,1,0:T(2,128)(2,1)S(1)}, u32[]{:S(2)}, u32[]{:S(2)}) async-start(bf16[16,2,2048]{2,1,0:T(2,128)(2,1)} %reshape.95), calls=%async_computation.2 | async-start | bytes 262144 | tf_op jit(solution)/shard_map/all_to_all | solution.py:134
  115.6 0.0 all-gather.2.cloned.1.call-start
  115.6 0.2 reshape.98
  115.9 0.2 copy.41
  116.1 0.2 reshape.84
  116.3 8.2 %all-to-all-done.2 = bf16[16,2,2048]{2,1,0:T(2,128)(2,1)S(1)} async-done(((bf16[16,2,2048]{2,1,0:T(2,128)(2,1)}), bf16[16,2,2048]{2,1,0:T(2,128)(2,1)S(1)}, u32[]{:S(2)}, u32[]{:S(2)}) %all-to-all-start.2) | async-done | bytes 131104 | tf_op jit(solution)/shard_map/all_to_all | solution.py:134
  124.5 0.2 reshape.96
  124.8 0.2 copy.37
  125.0 0.2 reshape.83
  125.2 1.2 fusion.44
  126.4 1.2 fusion.32
  127.6 0.1 copy.43
  127.7 0.7 convert_element_type.119
  128.5 32.2 %all-gather.2.cloned.1.call-done = bf16[16,1024,1,64]{1,3,2,0:T(8,128)(2,1)} async-done(((bf16[1,1024,1,64]{1,3,2,0:T(8,128)(2,1)}), bf16[16,1024,1,64]{1,3,2,0:T(8,128)(2,1)}) %all-gather.2.cloned.1.call-update) | async-done | bytes 2097168 | tf_op jit(solution)/shard_map/all_gather | solution.py:160
  160.7 3.0 %convolution_convert_fusion = bf16[1024,128]{1,0:T(8,128)(2,1)} fusion(bf16[1024,1024]{0,1:T(8,128)(2,1)} %bitcast.92, bf16[1024,128]{1,0:T(8,128)(2,1)S(1)} %copy-done), kind=kOutput, calls=%fused_computation.34 | convolution fusion | flops 268566528 | bytes 2621440 | tf_op jit(solution)/shard_map/dot_general | solution.py:162
  (16 shorter events, 0.2 us)
Async XLA Ops:
  6.5 154.2 %copy-start = (bf16[1024,128]{1,0:T(8,128)(2,1)S(1)}, bf16[1024,128]{1,0:T(8,128)(2,1)}, u32[]{:S(2)}) copy-start(bf16[1024,128]{1,0:T(8,128)(2,1)} %param.7) | copy-start | bytes 786436
  6.5 3.5 %copy-start.1 = (bf16[1024,2048]{1,0:T(8,128)(2,1)S(1)}, bf16[1024,2048]{1,0:T(8,128)(2,1)}, u32[]{:S(2)}) copy-start(bf16[1024,2048]{1,0:T(8,128)(2,1)} %param.4) | copy-start | bytes 12582916
  6.5 3.5 %copy-start.2 = (f32[2048]{0:T(1024)S(1)}, f32[2048]{0:T(1024)}, u32[]{:S(2)}) copy-start(f32[2048]{0:T(1024)} %param.5) | copy-start | bytes 24580
  14.3 23.1 %all-to-all-start = ((bf16[32,2,1024]{2,1,0:T(2,128)(2,1)}), bf16[32,2,1024]{2,1,0:T(2,128)(2,1)S(1)}, u32[]{:S(2)}, u32[]{:S(2)}) async-start(bf16[32,2,1024]{2,1,0:T(2,128)(2,1)} %reshape.91), calls=%async_computation | async-start | bytes 262144 | tf_op jit(solution)/shard_map/all_to_all | solution.py:92
  92.4 19.8 %all-to-all-start.3 = ((bf16[16,2,2048]{2,1,0:T(2,128)(2,1)}), bf16[16,2,2048]{2,1,0:T(2,128)(2,1)S(1)}, u32[]{:S(2)}, u32[]{:S(2)}) async-start(bf16[16,2,2048]{2,1,0:T(2,128)(2,1)} %reshape.97), calls=%async_computation.3 | async-start | bytes 262144 | tf_op jit(solution)/shard_map/all_to_all | solution.py:141
  112.2 12.3 %all-to-all-start.2 = ((bf16[16,2,2048]{2,1,0:T(2,128)(2,1)}), bf16[16,2,2048]{2,1,0:T(2,128)(2,1)S(1)}, u32[]{:S(2)}, u32[]{:S(2)}) async-start(bf16[16,2,2048]{2,1,0:T(2,128)(2,1)} %reshape.95), calls=%async_computation.2 | async-start | bytes 262144 | tf_op jit(solution)/shard_map/all_to_all | solution.py:134
  115.6 45.1 %all-gather.2.cloned.1.call-start = ((), (), s32[]{:S(2)}) async-start(), calls=%async_computation.4 | async-start | bytes 2228224 | tf_op jit(solution)/shard_map/all_gather | solution.py:160
Sparse Core Ops, SparseCore 0:
  128.6 32.0 all-gather.1
